TPU v7x, 32 devices: a whole 2x2x4 slice. The times are simulated.
32 devices in a mesh: sp: 8 (over z, y), tp: 4 (over x, core).
Axes of the slice: x: 2, y: 2, z: 4, core: 2. Of those that a mesh axis runs over, the one named last changes fastest.
Arguments:
- resid: bfloat16 [1024, 2048], P('sp', 'tp'), may hold values from -10.2 to 10.2
- query: bfloat16 [1024, 1024], P('sp', 'tp'), may hold values from -6 to 6
- memory_keys: bfloat16 [1024, 1024], P('sp', 'tp'), may hold values from -6 to 6
- value: bfloat16 [1024, 1024], P('sp', 'tp'), may hold values from -6 to 6
- output_gate_logits: bfloat16 [1024, 1024], P('sp', 'tp'), may hold values from -6 to 6
- gate_preactivation: float32 [4, 8, 1024], P(None, 'tp', 'sp'), may hold values from -6 to 96
- extra_forget_logs: float32 [2, 8, 1024], P(None, 'tp', 'sp'), may hold values from -0.7 to 0
- head_norm_gain: bfloat16 [1024], P('tp'), may hold values from 0.099609375 to 1.8984375
- output_weight: bfloat16 [1024, 2048], P('tp'), may hold values from -0.25 to 0.25
- mixer_norm_gain: bfloat16 [2048], P('tp'), may hold values from 0.099609375 to 1.8984375
- gate_up_weight: bfloat16 [2048, 5632], P('sp', 'tp'), may hold values from -0.125 to 0.125
- value_up_weight: bfloat16 [2048, 5632], P('sp', 'tp'), may hold values from -0.125 to 0.125
- convolution_weight: float32 [3, 5632], P(None, 'tp'), may hold values from -3 to 3
- down_weight: bfloat16 [5632, 2048], P('tp', 'sp'), may hold values from -0.109375 to 0.109375
Outputs:
- out: bfloat16 [1024, 2048], P('sp', 'tp')
All inputs are finite; a program needn't handle non-finite values.
Results may differ from a plain program's by a relative error of at most 0.02.
Values may be sent and summed in bfloat16 or wider, within the bound.
A program may use at most 128 MiB of HBM per device.

v0:
```python
import jax
import jax.numpy as jnp
from jax import lax
from jax.sharding import PartitionSpec as P

D = 2048
DH = 128
BLOCK = 64


NEG = -1e30
EPS = 1e-06
HIGH = lax.Precision.HIGHEST


def entering(array, axis, combine, identity, reverse):
    size, here = (lax.axis_size(axis), lax.axis_index(axis))
    everything = jax.tree.map(lambda part: lax.all_gather(part, axis), array)
    start = jax.tree.map(
        lambda part, zero: jnp.broadcast_to(jnp.asarray(zero, part.dtype), part.shape),
        array,
        identity,
    )

    def lap(k, before):
        at = size - 1 - k if reverse else k
        reached = at > here if reverse else at < here
        new = combine(before, jax.tree.map(lambda part: part[at], everything))
        return jax.tree.map(lambda a, b: jnp.where(reached, a, b), new, before)

    return lax.fori_loop(0, size, lap, start)


def extended(array, sides, width):
    for axis, dim in sides:
        size, length = (lax.axis_size(axis), array.shape[dim])
        up = [(i, (i + 1) % size) for i in range(size - 1)]
        down = [(j, i) for i, j in up]
        last = lax.slice_in_dim(array, length - width, length, axis=dim)
        first = lax.slice_in_dim(array, 0, width, axis=dim)
        before = lax.ppermute(last, axis, up)
        after = lax.ppermute(first, axis, down)
        array = jnp.concatenate([before, array, after], axis=dim)
    return array


def heads_blocks(source, head_count):
    length = source.shape[0]
    shaped = source.astype(jnp.float32).reshape(length // BLOCK, BLOCK, head_count, DH)
    return shaped.transpose(2, 0, 1, 3)


def merge_states(earlier, later):
    c_early, m_early, b_early = earlier
    c_late, m_late, b_late = later
    m_new = jnp.maximum(b_late + m_early, m_late)
    c_new = (
        jnp.exp(b_late + m_early - m_new)[..., None, None] * c_early
        + jnp.exp(m_late - m_new)[..., None, None] * c_late
    )
    return (c_new, m_new, b_early + b_late)


def carry_step(carry, inputs):
    return (merge_states(carry, inputs), carry)


def block_terms(key_rows, values, log_in, log_forget):
    cumulative = jnp.cumsum(log_forget, axis=-1)
    block_end = cumulative[..., -1]
    weight_log = block_end[..., None] - cumulative + log_in
    m_local = jnp.max(weight_log, axis=-1)
    weights = jnp.exp(weight_log - m_local[..., None])
    c_local = jnp.einsum("hnsd,hnse->hnde", weights[..., None] * key_rows, values, precision=HIGH)
    return (cumulative, block_end, m_local, c_local)


def block_output(queries, key_rows, values, log_in, cumulative, c_start, m_start):
    a_log = cumulative + m_start[..., None]
    d_log = cumulative[..., :, None] - cumulative[..., None, :] + log_in[..., None, :]
    block_len = cumulative.shape[-1]
    lower_mask = jnp.arange(block_len)[:, None] >= jnp.arange(block_len)[None, :]
    d_log = jnp.where(lower_mask, d_log, -jnp.inf)
    m_row = jnp.maximum(a_log, jnp.max(d_log, axis=-1))
    decays = jnp.exp(d_log - m_row[..., None])
    carried = jnp.exp(a_log - m_row)
    scores = jnp.einsum("hntd,hnsd->hnts", queries, key_rows, precision=HIGH) * decays
    numerator = jnp.einsum("hnts,hnse->hnte", scores, values, precision=HIGH) + carried[
        ..., None
    ] * jnp.einsum("hntd,hnde->hnte", queries, c_start, precision=HIGH)
    return (numerator, m_row)


def single_direction(query, memory_keys, value, log_in, log_forget, reverse):
    head_count = query.shape[1] // DH
    nblocks = query.shape[0] // BLOCK
    queries = heads_blocks(query, head_count)
    key_rows = heads_blocks(memory_keys, head_count) * DH ** (-0.5)
    values = heads_blocks(value, head_count)
    log_in = log_in.reshape(head_count, nblocks, BLOCK)
    log_forget = log_forget.reshape(head_count, nblocks, BLOCK)
    cumulative, block_end, m_local, c_local = block_terms(key_rows, values, log_in, log_forget)
    identity = (
        jnp.zeros((head_count, DH, DH), jnp.float32),
        jnp.full((head_count,), NEG, jnp.float32),
        jnp.zeros((head_count,), jnp.float32),
    )
    totals, prefix = lax.scan(
        carry_step, identity, (jnp.moveaxis(c_local, 1, 0), m_local.T, block_end.T)
    )
    if reverse:
        incoming = entering(totals, "sp", merge_states, identity, True)
    else:
        incoming = entering(totals, "sp", merge_states, identity, False)
    starts = merge_states(tuple((member[None] for member in incoming)), prefix)
    c_start = jnp.moveaxis(starts[0], 0, 1)
    m_start = starts[1].T
    numerator, m_row = block_output(queries, key_rows, values, log_in, cumulative, c_start, m_start)
    return (numerator.reshape(head_count, -1, DH), m_row.reshape(head_count, -1))


def per_device(
    resid,
    query,
    memory_keys,
    value,
    output_gate_logits,
    gate_preactivation,
    extra_forget_logs,
    head_norm_gain,
    output_weight,
    mixer_norm_gain,
    gate_up_weight,
    value_up_weight,
    convolution_weight,
    down_weight,
):
    tokens = query.shape[0]
    forward_numerator, forward_peak = single_direction(
        query,
        memory_keys,
        value,
        gate_preactivation[0],
        jax.nn.log_sigmoid(gate_preactivation[1]) + extra_forget_logs[0],
        False,
    )
    backward_numerator, backward_peak = single_direction(
        jnp.flip(query, 0),
        jnp.flip(memory_keys, 0),
        jnp.flip(value, 0),
        jnp.flip(gate_preactivation[2], -1),
        jnp.flip(jax.nn.log_sigmoid(gate_preactivation[3]) + extra_forget_logs[1], -1),
        True,
    )
    backward_numerator = jnp.flip(backward_numerator, 1)
    backward_peak = jnp.flip(backward_peak, 1)
    both_max = jnp.maximum(forward_peak, backward_peak)
    numerator = (
        jnp.exp(forward_peak - both_max)[..., None] * forward_numerator
        + jnp.exp(backward_peak - both_max)[..., None] * backward_numerator
    )
    normal_cell = numerator * lax.rsqrt(
        jnp.mean(numerator * numerator, axis=-1, keepdims=True) + EPS
    )
    cell = normal_cell.transpose(1, 0, 2).reshape(tokens, -1)
    cell = (
        cell
        * head_norm_gain.astype(jnp.float32)
        * jax.nn.sigmoid(output_gate_logits.astype(jnp.float32))
    ).astype(jnp.bfloat16)
    partial_proj = jnp.dot(cell, output_weight, preferred_element_type=jnp.float32)
    stream = (
        resid.astype(jnp.float32)
        + lax.psum_scatter(
            partial_proj.astype(jnp.bfloat16), "tp", scatter_dimension=1, tiled=True
        ).astype(jnp.float32)
    ).astype(jnp.bfloat16)
    stream_f = stream.astype(jnp.float32)
    squares = lax.psum(jnp.sum(stream_f * stream_f, axis=1), "tp")
    normed_own = (
        stream_f * lax.rsqrt(squares / D + EPS)[:, None] * mixer_norm_gain.astype(jnp.float32)
    ).astype(jnp.bfloat16)
    normed = lax.all_gather(normed_own, "tp", axis=1, tiled=True)
    gate_sum = jnp.dot(
        normed,
        lax.all_gather(gate_up_weight, "sp", axis=0, tiled=True),
        preferred_element_type=jnp.float32,
    )
    value_sum = jnp.dot(
        normed,
        lax.all_gather(value_up_weight, "sp", axis=0, tiled=True),
        preferred_element_type=jnp.float32,
    )
    gate_mix = gate_sum.astype(jnp.bfloat16)
    value_mix = value_sum.astype(jnp.bfloat16)
    padded = extended(gate_mix, (("sp", 0),), 1)
    padded_f = padded.astype(jnp.float32)
    convolved = (
        convolution_weight[0] * padded_f[:-2]
        + convolution_weight[1] * padded_f[1:-1]
        + convolution_weight[2] * padded_f[2:]
    )
    hidden = (jax.nn.gelu(convolved) * value_mix.astype(jnp.float32)).astype(jnp.bfloat16)
    down_term = jnp.dot(
        hidden,
        lax.all_gather(down_weight, "sp", axis=1, tiled=True),
        preferred_element_type=jnp.float32,
    )
    mixer_out = lax.psum_scatter(
        down_term.astype(jnp.bfloat16), "tp", scatter_dimension=1, tiled=True
    ).astype(jnp.float32)
    return (stream.astype(jnp.float32) + mixer_out).astype(jnp.bfloat16)


def solution(mesh):
    return jax.shard_map(
        per_device,
        mesh=mesh,
        in_specs=(
            P("sp", "tp"),
            P("sp", "tp"),
            P("sp", "tp"),
            P("sp", "tp"),
            P("sp", "tp"),
            P(None, "tp", "sp"),
            P(None, "tp", "sp"),
            P("tp"),
            P("tp", None),
            P("tp"),
            P("sp", "tp"),
            P("sp", "tp"),
            P(None, "tp"),
            P("tp", "sp"),
        ),
        out_specs=P("sp", "tp"),
        check_vma=False,
    )
```

profile of v0, /device:TPU:29, one launch (start us, length us, event | category | flops | bytes accessed | tf_op | source)
XLA Modules:
  0.0 445.7 jit_solution(8462762359429612911)
XLA Ops:
  20.7 13.5 %all-reduce.4 = (f32[16]{0:T(128)S(1)}, f32[16]{0:T(128)S(1)}, f32[16]{0:T(128)S(1)}, f32[16]{0:T(128)S(1)}) all-reduce(f32[16]{0:T(128)S(1)} %dynamic-update-slice.2, f32[16]{0:T(128)S(1)} %dynamic-update-slice.3, f32[16]{0:T(128)S(1)} %dynamic-update-slice, f32[16]{0:T(128)S(1)} %dynamic-update-slice.1), channel_id=5, replica_groups=mesh['sp'=8,'tp'=4] {'sp'}, use_global_device_ids=true, to_apply=%add.2 | all-reduce | flops 64 | bytes 512
  34.8 17.2 %all-gather.18.cloned.1.call-done = f32[16,128,128]{2,1,0:T(8,128)} async-done(((f32[2,128,128]{2,1,0:T(8,128)}), f32[16,128,128]{2,1,0:T(8,128)}) %all-gather.18.cloned.1.call-update) | async-done | bytes 1048592 | tf_op jit(solution)/shard_map/all_gather | solution.py:18
  52.0 8.5 %while.77 = (s32[]{:T(128)}, f32[2,128,128]{2,1,0:T(8,128)S(1)}, f32[2]{0:T(128)S(1)}, s32[]{:T(128)}, f32[8,2]{1,0:T(8,128)S(1)}, /*index=5*/f32[8,2]{1,0:T(8,1...) while((s32[]{:T(128)}, f32[2,128,128]{2,1,0:T(8,128)S(1)}, f32[2]{0:T(128)S(1)}, s32[]{:T(128)}, ...), condition=%wide.region_5.6_spmd.clone, body=%wide.region_4.5_spmd.clone.sunk | while | flops 163858 | bytes 393431 | solution.py:31
  61.1 32.1 %all-gather.20.cloned.1.call-done = f32[16,128,128]{2,1,0:T(8,128)} async-done(((f32[2,128,128]{2,1,0:T(8,128)}), f32[16,128,128]{2,1,0:T(8,128)}) %all-gather.20.cloned.1.call-update) | async-done | bytes 1048592 | tf_op jit(solution)/shard_map/all_gather | solution.py:18
  93.2 8.6 %while.79 = (s32[]{:T(128)}, f32[2,128,128]{2,1,0:T(8,128)S(1)}, f32[2]{0:T(128)S(1)}, s32[]{:T(128)}, f32[8,2]{1,0:T(8,128)S(1)}, /*index=5*/f32[8,2]{1,0:T(8,1...) while((s32[]{:T(128)}, f32[2,128,128]{2,1,0:T(8,128)S(1)}, ...), condition=%wide.region_12.13_spmd.clone, body=%wide.region_11.12_spmd.clone.sunk | while | flops 163862 | bytes 393493 | solution.py:31
  94.3 1.0 fusion.133
  96.4 1.0 fusion.133
  98.6 1.0 fusion.133
  100.7 1.0 fusion.133
  104.2 1.1 convolution_convert_fusion
  107.1 22.6 %reduce-scatter.3.cloned.1.call-done = bf16[128,512]{1,0:T(8,128)(2,1)} async-done(((bf16[128,2048]{1,0:T(8,128)(2,1)}), bf16[128,512]{1,0:T(8,128)(2,1)}) %reduce-scatter.3.cloned.1.call-update) | async-done | bytes 131088 | tf_op jit(solution)/shard_map/reduce_scatter | solution.py:174
  129.7 1.0 fusion.49
  130.8 5.9 %psum.7 = f32[128]{0:T(128)S(1)} all-reduce(f32[128]{0:T(128)S(1)} %fusion.49), channel_id=1, replica_groups=mesh['sp'=8,'tp'=4] {'tp'}, use_global_device_ids=true, to_apply=%region_17.18 | all-reduce | flops 128 | bytes 1024 | tf_op jit(solution)/shard_map/psum | solution.py:179
  136.6 1.0 fusion.51
  137.6 7.4 %all_gather.60 = bf16[128,2048]{1,0:T(8,128)(2,1)S(1)} all-gather(bf16[128,512]{1,0:T(8,128)(2,1)S(1)} %fusion.51), channel_id=1, replica_groups=mesh['sp'=8,'tp'=4] {'tp'}, dimensions={1}, use_global_device_ids=true | all-gather | bytes 655360 | tf_op jit(solution)/shard_map/all_gather | solution.py:183
  145.1 76.5 %all-gather.12.cloned.1.call-done = bf16[2048,1408]{1,0:T(8,128)(2,1)} async-done(((bf16[256,1408]{1,0:T(8,128)(2,1)}), bf16[2048,1408]{1,0:T(8,128)(2,1)}) %all-gather.12.cloned.1.call-update) | async-done | bytes 5767184 | tf_op jit(solution)/shard_map/all_gather | solution.py:186
  221.5 3.6 convolution_convert_fusion.3
  225.2 1.3 collective-permute-start
  226.5 4.0 collective-permute-start.1
  231.3 82.8 %all-gather.14.cloned.1.call-done = bf16[2048,1408]{1,0:T(8,128)(2,1)} async-done(((bf16[256,1408]{1,0:T(8,128)(2,1)}), bf16[2048,1408]{1,0:T(8,128)(2,1)}) %all-gather.14.cloned.1.call-update) | async-done | bytes 5767184 | tf_op jit(solution)/shard_map/all_gather | solution.py:191
  314.1 93.2 %all-gather.16.cloned.1.call-done = bf16[1408,2048]{1,0:T(8,128)(2,1)} async-done(((bf16[1408,256]{1,0:T(8,128)(2,1)}), bf16[1408,2048]{1,0:T(8,128)(2,1)}) %all-gather.16.cloned.1.call-update) | async-done | bytes 5767184 | tf_op jit(solution)/shard_map/all_gather | solution.py:206
  407.3 7.3 %convolution_convert_fusion.1 = bf16[128,2048]{1,0:T(8,128)(2,1)} fusion(bf16[1408,2048]{1,0:T(8,128)(2,1)} %all-gather.16.cloned.1.call-done, bf16[128,2048]{1,0:T(8,128)(2,1)S(1)} %all_gather.60, bf16[2048,1408]{1,0:T(8,128)(2,1)} %all-gather.14.cloned.1.call-done, f32[130,1408]{1,0:T(8,128)S(1)} %maximum_convert_fusion, ...), kind=kOutput, calls=%fused_computation.57 | convolution fusion | flops 1479720960 | bytes 14770176 | tf_op jit(solution)/shard_map/dot_general | solution.py:204
  414.7 22.6 %reduce-scatter.5.cloned.1.call-done = bf16[128,512]{1,0:T(8,128)(2,1)} async-done(((bf16[128,2048]{1,0:T(8,128)(2,1)}), bf16[128,512]{1,0:T(8,128)(2,1)}) %reduce-scatter.5.cloned.1.call-update) | async-done | bytes 131088 | tf_op jit(solution)/shard_map/reduce_scatter | solution.py:209
  437.3 1.6 fusion.52
  (202 shorter events, 32.8 us)
Async XLA Ops:
  6.5 97.6 %copy-start = (bf16[256,2048]{1,0:T(8,128)(2,1)S(1)}, bf16[256,2048]{1,0:T(8,128)(2,1)}, u32[]{:S(2)}) copy-start(bf16[256,2048]{1,0:T(8,128)(2,1)} %param.30) | copy-start | bytes 3145732
  6.5 12.1 %copy-start.10 = (u32[32]{0:T(128)S(1)}, u32[32]{0:T(128)}, u32[]{:S(2)}) copy-start(u32[32]{0:T(128)} %constant.140) | copy-start | bytes 388
  6.5 12.0 %copy-start.5 = (bf16[128,256]{1,0:T(8,128)(2,1)S(1)}, bf16[128,256]{1,0:T(8,128)(2,1)}, u32[]{:S(2)}) copy-start(bf16[128,256]{1,0:T(8,128)(2,1)} %param.23) | copy-start | bytes 196612
  6.5 28.2 %copy-start.9 = (bf16[256]{0:T(256)(128)(2,1)S(1)}, bf16[256]{0:T(256)(128)(2,1)}, u32[]{:S(2)}) copy-start(bf16[256]{0:T(256)(128)(2,1)} %param.29) | copy-start | bytes 1540
  6.5 45.5 %all-gather.18.cloned.1.call-start = ((), (), s32[]{:S(2)}) async-start(), calls=%async_computation.7 | async-start | bytes 1179648 | tf_op jit(solution)/shard_map/all_gather | solution.py:18
  14.0 0.7 copy-start.1
  14.6 78.5 %all-gather.20.cloned.1.call-start = ((), (), s32[]{:S(2)}) async-start(), calls=%async_computation.8 | async-start | bytes 1179648 | tf_op jit(solution)/shard_map/all_gather | solution.py:18
  17.3 86.9 %copy-start.6 = (bf16[128,256]{1,0:T(8,128)(2,1)S(1)}, bf16[128,256]{1,0:T(8,128)(2,1)}, u32[]{:S(2)}) copy-start(bf16[128,256]{1,0:T(8,128)(2,1)} %param.26) | copy-start | bytes 196612
  17.8 0.7 copy-start.2
  18.5 111.3 %reduce-scatter.3.cloned.1.call-start = ((), (), s32[]{:S(2)}) async-start(), calls=%async_computation.2 | async-start | bytes 655360 | tf_op jit(solution)/shard_map/reduce_scatter | solution.py:174
  60.5 46.6 %copy-start.8 = (bf16[512]{0:T(512)(128)(2,1)S(1)}, bf16[512]{0:T(512)(128)(2,1)}, u32[]{:S(2)}) copy-start(bf16[512]{0:T(512)(128)(2,1)} %param.31) | copy-start | bytes 3076
  60.5 69.2 %copy-start.3 = (bf16[128,512]{1,0:T(8,128)(2,1)S(1)}, bf16[128,512]{1,0:T(8,128)(2,1)}, u32[]{:S(2)}) copy-start(bf16[128,512]{1,0:T(8,128)(2,1)} %param.22) | copy-start | bytes 393220
  105.3 125.2 %copy-start.7 = (f32[3,1408]{1,0:T(4,128)S(1)}, f32[3,1408]{1,0:T(4,128)}, u32[]{:S(2)}) copy-start(f32[3,1408]{1,0:T(4,128)} %param.34) | copy-start | bytes 50692
  105.3 116.2 %all-gather.12.cloned.1.call-start = ((), (), s32[]{:S(2)}) async-start(), calls=%async_computation.3 | async-start | bytes 6488064 | tf_op jit(solution)/shard_map/all_gather | solution.py:186
  105.9 208.2 %all-gather.14.cloned.1.call-start = ((), (), s32[]{:S(2)}) async-start(), calls=%async_computation.4 | async-start | bytes 6488064 | tf_op jit(solution)/shard_map/all_gather | solution.py:191
  106.5 300.9 %all-gather.16.cloned.1.call-start = ((), (), s32[]{:S(2)}) async-start(), calls=%async_computation.5 | async-start | bytes 6488064 | tf_op jit(solution)/shard_map/all_gather | solution.py:206
  107.1 330.2 %reduce-scatter.5.cloned.1.call-start = ((), (), s32[]{:S(2)}) async-start(), calls=%async_computation.6 | async-start | bytes 655360 | tf_op jit(solution)/shard_map/reduce_scatter | solution.py:209
  225.2 5.4 %collective-permute-start = (bf16[1,1408]{1,0:T(2,128)(2,1)S(1)}, bf16[1,1408]{1,0:T(2,128)(2,1)S(1)}, u32[]{:S(2)}, u32[]{:S(2)}) collective-permute-start(bf16[1,1408]{1,0:T(2,128)(2,1)S(1)} %get-tuple-element.704), channel_id=1, source_target_pairs={{0,4},{4,8},{8,12},{12,16},{16,20},{20,24},{24,28},{1,5},{5,9},{9,... | collective-permute-start | bytes 8456 | tf_op jit(solution)/shard_map/ppermute | solution.py:41
  226.5 4.7 %collective-permute-start.1 = (bf16[1,1408]{1,0:T(2,128)(2,1)S(1)}, bf16[1,1408]{1,0:T(2,128)(2,1)S(1)}, u32[]{:S(2)}, u32[]{:S(2)}) collective-permute-start(bf16[1,1408]{1,0:T(2,128)(2,1)S(1)} %get-tuple-element.705), channel_id=1, source_target_pairs={{4,0},{8,4},{12,8},{16,12},{20,16},{24,20},{28,24},{5,1},{9,5},{13... | collective-permute-start | bytes 8456 | tf_op jit(solution)/shard_map/ppermute | solution.py:42
  407.3 29.9 %copy-start.4 = (bf16[128,512]{1,0:T(8,128)(2,1)S(1)}, bf16[128,512]{1,0:T(8,128)(2,1)}, u32[]{:S(2)}) copy-start(bf16[128,512]{1,0:T(8,128)(2,1)} %reduce-scatter.3.cloned.1.call-done) | copy-start | bytes 393220
Sparse Core Ops, SparseCore 0:
  14.8 37.2 all-gather.17
  54.1 38.9 all-gather.19
  105.4 24.2 reduce-scatter.2
  131.8 89.7 all-gather.11
  223.6 90.4 all-gather.13
  316.0 91.2 all-gather.15
  414.8 22.3 reduce-scatter.4
where the time goes:
time: 449 us; the launch traced here: 446 us
  waiting for transfers between devices  349 us (78%)
  blocking collectives  26.8 us (6%)
  other arithmetic  24.5 us (5%)
  matrix products  14.7 us (3%)
  between operations  14.6 us (3%)
  local copies, waits for them, and re-layouts  9.61 us (2%)
  starting transfers between devices  5.55 us (1%)
    all_gather x1, waiting for transfers between devices, per_device(): lax.all_gather(down_weight, 'sp', axis=1, tiled=True)  93.2 us
    all_gather x1, waiting for transfers between devices, per_device(): lax.all_gather(value_up_weight, 'sp', axis=0, tiled=True)  82.8 us
    all_gather x1, waiting for transfers between devices, per_device(): lax.all_gather(gate_up_weight, 'sp', axis=0, tiled=True)  76.5 us
    all_gather x2, waiting for transfers between devices, entering(): everything = jax.tree.map(lambda part: lax.all_gather(part, axis), array)  49.3 us
    reduce_scatter x1, waiting for transfers between devices, per_device(): lax.psum_scatter(partial_proj.astype(jnp.bfloat16), 'tp', scatter_dimensi...  22.6 us
    reduce_scatter x1, waiting for transfers between devices, per_device(): lax.psum_scatter(down_term.astype(jnp.bfloat16), 'tp', scatter_dimension=...  22.6 us
    select_n x32, other arithmetic, lap(): return jax.tree.map(lambda a, b: jnp.where(reached, a, b), new, before)  16.3 us
    unnamed x1, blocking collectives  13.5 us
  transfers between devices with their start and end apart: 9, of which 8 were waited for; matrix products, arithmetic and copies ran while one was open for 4% of the time, Pallas kernels for 0%

commit v1 on v0

--- a/solution.py
+++ b/solution.py
@@ -1,6 +1,10 @@
+import functools
+
 import jax
 import jax.numpy as jnp
 from jax import lax
+from jax.experimental import pallas as pl
+from jax.experimental.pallas import tpu as pltpu
 from jax.sharding import PartitionSpec as P
 
 D = 2048
@@ -212,9 +216,635 @@
     return (stream.astype(jnp.float32) + mixer_out).astype(jnp.bfloat16)
 
 
+LANE = 128
+MESH = pl.DeviceIdType.MESH
+F32 = jnp.float32
+BF16 = jnp.bfloat16
+
+
+def remote(src, dst, send, recv, sp, tp):
+    return pltpu.make_async_remote_copy(
+        src_ref=src,
+        dst_ref=dst,
+        send_sem=send,
+        recv_sem=recv,
+        device_id=(sp, tp),
+        device_id_type=MESH,
+    )
+
+
+def nt_dot(a, b, precision=None):
+    return lax.dot_general(
+        a, b, (((1,), (1,)), ((), ())), precision=precision, preferred_element_type=F32
+    )
+
+
+def layer_kernel(
+    n_sp,
+    n_tp,
+    resid,
+    query,
+    keys,
+    value,
+    gate_logits,
+    gates,
+    extra_logs,
+    head_gain,
+    out_w,
+    mixer_gain,
+    gate_w,
+    value_w,
+    taps,
+    down_w,
+    out,
+    k_all,
+    v_all,
+    g_own,
+    g_all,
+    lf_own,
+    wo_all,
+    taps_all,
+    gain_own,
+    gain_all,
+    w_up,
+    w_down,
+    cell_own,
+    cell_all,
+    stream_own,
+    x_all,
+    gate_buf,
+    value_buf,
+    halo,
+    hidden_buf,
+    part,
+    r_all,
+    k_sem,
+    v_sem,
+    g_sem,
+    wo_sem,
+    taps_sem,
+    gain_sem,
+    wg_sem,
+    wv_sem,
+    wd_sem,
+    xg_sem,
+    xv_sem,
+    xd_sem,
+    fwd_sem,
+    cell_sem,
+    x_send,
+    x_recv,
+    halo_sem,
+    r_send,
+    r_recv,
+    local_sem,
+    local_x,
+):
+    s, t = (lax.axis_index("sp"), lax.axis_index("tp"))
+    core = lax.rem(t, 2)
+    pair = t // 2
+    partner = t + 1 - 2 * core
+    n_pair = n_tp // 2
+    tokens = query.shape[0]
+    width = query.shape[1]
+    features = resid.shape[1]
+    depth = gate_w.shape[0]
+    cols = down_w.shape[1]
+    heads = width // DH
+    tiles = gate_w.shape[1] // LANE
+    extras = tiles - n_sp
+    half = n_sp // 2
+    my_half = s // half
+    model = features * n_tp
+
+    def loop(low, high, body):
+        def step(i, carry):
+            body(i)
+            return carry
+
+        lax.fori_loop(low, high, step, 0)
+
+    rows = lambda i: pl.ds(pl.multiple_of(i * tokens, tokens), tokens)
+    lanes = lambda i, size: pl.ds(pl.multiple_of(i * size, LANE), size)
+    drows = lambda i: pl.ds(pl.multiple_of(i * depth, depth), depth)
+    trows = lambda i: pl.ds(pl.multiple_of(i * LANE, LANE), LANE)
+
+    def kv_copies(d):
+        to = lax.rem(s + d, n_sp)
+        return (
+            remote(keys, k_all.at[rows(s), :], k_sem.at[0, d], k_sem.at[1, d], to, t),
+            remote(value, v_all.at[rows(s), :], v_sem.at[0, d], v_sem.at[1, d], to, t),
+        )
+
+    def g_copy(d):
+        to = lax.rem(s + d, n_sp)
+        return remote(g_own, g_all.at[s], g_sem.at[0, d], g_sem.at[1, d], to, t)
+
+    def wo_copy(e):
+        to = lax.rem(t + e, n_tp)
+        return remote(
+            out_w.at[:, lanes(to, features)],
+            wo_all.at[pl.ds(pl.multiple_of(t * width, width), width), :],
+            wo_sem.at[0, e],
+            wo_sem.at[1, e],
+            s,
+            to,
+        )
+
+    def gain_copy(e):
+        to = lax.rem(t + e, n_tp)
+        return remote(
+            gain_own, gain_all.at[:, lanes(t, features)], gain_sem.at[0, e], gain_sem.at[1, e], s, to
+        )
+
+    def taps_copy():
+        return remote(taps, taps_all.at[core], taps_sem.at[0], taps_sem.at[1], s, partner)
+
+    def tile_ends(tile, slot):
+        return (
+            (gate_w.at[:, lanes(tile, LANE)], w_up.at[slot, drows(s), pl.ds(0, LANE)]),
+            (value_w.at[:, lanes(tile, LANE)], w_up.at[slot, drows(s), pl.ds(LANE, LANE)]),
+            (down_w.at[trows(tile), :], w_down.at[trows(slot), lanes(s, cols)]),
+        )
+
+    def weight_copies(d):
+        to = lax.rem(s + d, n_sp)
+        sems = (wg_sem, wv_sem, wd_sem)
+        return tuple(
+            remote(a, b, sem.at[0, d], sem.at[1, d], to, t)
+            for (a, b), sem in zip(tile_ends(to, core), sems)
+        )
+
+    def extra_copies(e, source):
+        to = e + extras * core
+        sems = (xg_sem, xv_sem, xd_sem)
+        return tuple(
+            remote(a, b, sem.at[0, e], sem.at[1, source], to, t)
+            for (a, b), sem in zip(tile_ends(n_sp + e, 2), sems)
+        )
+
+    def local_copies():
+        pairs = (
+            (keys, k_all.at[rows(s), :]),
+            (value, v_all.at[rows(s), :]),
+            (out_w.at[:, lanes(t, features)],
+             wo_all.at[pl.ds(pl.multiple_of(t * width, width), width), :]),
+        ) + tile_ends(s, core)
+        return tuple(
+            pltpu.make_async_copy(a, b, local_sem.at[i]) for i, (a, b) in enumerate(pairs)
+        )
+
+    def local_extra(e):
+        return tuple(
+            pltpu.make_async_copy(a, b, local_x.at[i])
+            for i, (a, b) in enumerate(tile_ends(n_sp + e, 2))
+        )
+
+    def start_kv(d):
+        for copy in kv_copies(d):
+            copy.start()
+
+    loop(1, n_sp, start_kv)
+    for copy in local_copies():
+        copy.start()
+
+    def log_sigmoid(x):
+        return jnp.minimum(x, 0.0) - jnp.log1p(jnp.exp(-jnp.abs(x)))
+
+    lf_own[...] = jnp.zeros_like(lf_own)
+    lf_own[0:heads, :] = log_sigmoid(gates[1]) + extra_logs[0]
+    lf_own[heads : 2 * heads, :] = log_sigmoid(gates[3]) + extra_logs[1]
+    lf = lf_own[...]
+    row_id = lax.broadcasted_iota(jnp.int32, (tokens, tokens), 0)
+    col_id = lax.broadcasted_iota(jnp.int32, (tokens, tokens), 1)
+    upto = (row_id >= col_id).astype(F32)
+    below = (row_id > col_id).astype(F32)
+    row_incl = nt_dot(lf, upto, HIGH)
+    row_excl = nt_dot(lf, below, HIGH)
+    col_incl = nt_dot(upto, lf, HIGH)
+    col_excl = nt_dot(below, lf, HIGH)
+    total = jnp.broadcast_to(jnp.sum(lf, axis=1, keepdims=True), lf.shape)
+    g_own[0:heads, :] = gates[0] - row_incl[0:heads]
+    g_own[heads : 2 * heads, :] = gates[2] + row_excl[heads : 2 * heads]
+    g_own[2 * heads : 4 * heads, :] = total[0 : 2 * heads]
+    gain_own[...] = jnp.broadcast_to(mixer_gain[...].astype(F32), gain_own.shape)
+    g_all[s] = g_own[...]
+    gain_all[:, lanes(t, features)] = gain_own[...]
+    taps_all[core] = taps[...]
+    loop(1, n_sp, lambda d: g_copy(d).start())
+
+    def start_tp(e):
+        wo_copy(e).start()
+        gain_copy(e).start()
+
+    loop(1, n_tp, start_tp)
+    taps_copy().start()
+
+    def start_weights(d):
+        for copy in weight_copies(d):
+            copy.start()
+
+    loop(1, n_sp, start_weights)
+
+    def start_extra(e):
+        @pl.when(e + extras * core != s)
+        def _():
+            for copy in extra_copies(e, s):
+                copy.start()
+
+        @pl.when(e + extras * core == s)
+        def _():
+            for copy in local_extra(e):
+                copy.start()
+
+    loop(0, extras, start_extra)
+
+    loop(1, n_sp, lambda d: g_copy(d).wait_recv())
+
+    def wait_kv(d):
+        for copy in kv_copies(d):
+            copy.wait_recv()
+
+    for copy in local_copies()[:3]:
+        copy.wait()
+    g = [g_all[j] for j in range(n_sp)]
+    diag_lower = row_id >= col_id
+    diag_upper = row_id <= col_id
+    logs, peaks = ([], [])
+    for h in range(heads):
+        acc = jnp.zeros((1, tokens), F32)
+        rows_f = [None] * n_sp
+        for j in reversed(range(n_sp)):
+            acc = acc + jnp.where(j < s, g[j][2 * heads + h : 2 * heads + h + 1], 0.0)
+            rows_f[j] = g[j][h : h + 1] + acc
+        acc = jnp.zeros((1, tokens), F32)
+        logs_h = []
+        f_col = col_incl[:, h : h + 1]
+        b_col = -col_excl[:, heads + h : heads + h + 1]
+        peak = jnp.full((tokens, 1), NEG, F32)
+        for j in range(n_sp):
+            row_b = g[j][heads + h : heads + h + 1] + acc
+            acc = acc + jnp.where(j >= s, g[j][3 * heads + h : 3 * heads + h + 1], 0.0)
+            fwd = jnp.where(jnp.logical_or(j < s, jnp.logical_and(j == s, diag_lower)), f_col + rows_f[j], NEG)
+            bwd = jnp.where(jnp.logical_or(j > s, jnp.logical_and(j == s, diag_upper)), b_col + row_b, NEG)
+            peak = jnp.maximum(peak, jnp.max(jnp.maximum(fwd, bwd), axis=1, keepdims=True))
+            logs_h.append((fwd, bwd))
+        peaks.append(peak)
+        logs.append(
+            jnp.concatenate([jnp.exp(f - peak) + jnp.exp(b - peak) for f, b in logs_h], axis=1)
+        )
+    loop(1, n_sp, wait_kv)
+    for h in range(heads):
+        lane = slice(h * DH, (h + 1) * DH)
+        scores = nt_dot(query[:, lane], k_all[:, lane]) * DH ** (-0.5)
+        weighted = (scores * logs[h]).astype(BF16)
+        numer = jnp.dot(weighted, v_all[:, lane], preferred_element_type=F32)
+        scale = lax.rsqrt(jnp.mean(numer * numer, axis=1, keepdims=True) + EPS)
+        gated = (
+            numer * scale * head_gain[:, lane].astype(F32)
+            * jax.nn.sigmoid(gate_logits[:, lane].astype(F32))
+        )
+        cell_own[:, lane] = gated.astype(BF16)
+
+    def cell_copy(e):
+        to = lax.rem(t + e, n_tp)
+        return remote(cell_own, cell_all.at[t], cell_sem.at[0, e], cell_sem.at[1, e], s, to)
+
+    loop(1, n_tp, lambda e: cell_copy(e).start())
+    cell_all[t] = cell_own[...]
+
+    def wait_tp(e):
+        wo_copy(e).wait_recv()
+        gain_copy(e).wait_recv()
+        cell_copy(e).wait_recv()
+
+    loop(1, n_tp, wait_tp)
+    projected = jnp.zeros((tokens, features), F32)
+    for m in range(n_tp):
+        piece = jnp.dot(
+            cell_all[m], wo_all[m * width : (m + 1) * width, :], preferred_element_type=F32
+        )
+        projected = projected + piece.astype(BF16).astype(F32)
+    stream_own[...] = (resid[...].astype(F32) + projected).astype(BF16)
+
+    place = lax.rem(s, half)
+
+    def x_copy(d):
+        chip = lax.rem(s * n_pair + pair + d, n_sp * n_pair)
+        to_s, to_t = (chip // n_pair, 2 * lax.rem(chip, n_pair) + my_half)
+        return to_s, to_t, remote(
+            stream_own,
+            x_all.at[place, :, lanes(t, features)],
+            x_send.at[d],
+            x_recv.at[place * n_tp + t],
+            to_s,
+            to_t,
+        )
+
+    def start_x(d):
+        to_s, to_t, copy = x_copy(d)
+        mine = jnp.logical_and(to_s == s, to_t == t)
+
+        @pl.when(jnp.logical_not(mine))
+        def _():
+            copy.start()
+
+        @pl.when(mine)
+        def _():
+            x_all[place, :, lanes(t, features)] = stream_own[...]
+
+    loop(0, n_sp * n_pair, start_x)
+
+    def wait_weights(d):
+        for copy in weight_copies(d):
+            copy.wait_recv()
+
+    loop(1, n_sp, wait_weights)
+    for copy in local_copies()[3:]:
+        copy.wait()
+    owner = jnp.logical_and(s >= extras * core, s < extras * (core + 1))
+    other_owner = jnp.logical_and(s >= extras * (1 - core), s < extras * (2 - core))
+
+    def forward_copies(slot, base):
+        return (
+            remote(w_up.at[slot], w_up.at[slot], fwd_sem.at[0, base], fwd_sem.at[1, base], s, partner),
+            remote(
+                w_down.at[trows(slot), :],
+                w_down.at[trows(slot), :],
+                fwd_sem.at[0, base + 1],
+                fwd_sem.at[1, base + 1],
+                s,
+                partner,
+            ),
+        )
+
+    for copy in forward_copies(core, 0):
+        copy.start()
+
+    @pl.when(owner)
+    def _():
+        def wait_extra(source):
+            @pl.when(source != s)
+            def _():
+                for copy in extra_copies(0, source):
+                    copy.wait_recv()
+
+        loop(0, n_sp, wait_extra)
+        for copy in local_extra(0):
+            copy.wait()
+        for copy in forward_copies(2, 2):
+            copy.start()
+
+    @pl.when(s >= 2 * extras)
+    def _():
+        w_up[2] = jnp.zeros(w_up.shape[1:], BF16)
+        w_down[2 * LANE :, :] = jnp.zeros((LANE, w_down.shape[1]), BF16)
+
+    taps_copy().wait_recv()
+    for copy in forward_copies(1 - core, 0):
+        copy.wait_recv()
+
+    @pl.when(other_owner)
+    def _():
+        for copy in forward_copies(2, 2):
+            copy.wait_recv()
+
+    def mix_block(j):
+        for m in range(n_tp):
+            mine = jnp.logical_and(core * half + j == s, t == m)
+
+            @pl.when(jnp.logical_not(mine))
+            def _(m=m):
+                remote(
+                    stream_own,
+                    x_all.at[j, :, pl.ds(m * features, features)],
+                    x_send.at[0],
+                    x_recv.at[j * n_tp + m],
+                    s,
+                    partner,
+                ).wait_recv()
+
+        x = x_all[j].astype(F32)
+        squares = jnp.sum(x * x, axis=1, keepdims=True)
+        normed = (x * lax.rsqrt(squares / model + EPS) * gain_all[0:1, :]).astype(BF16)
+        for slot in range(3):
+            both = jnp.dot(normed, w_up[slot], preferred_element_type=F32).astype(BF16)
+            lane = slice(slot * LANE, (slot + 1) * LANE)
+            gate_buf[rows(j), lane] = both[:, :LANE]
+            value_buf[rows(j), lane] = both[:, LANE:]
+
+    loop(0, half, mix_block)
+
+    count = half * tokens
+    edge = halo.shape[0]
+
+    def halo_copy():
+        start = pl.multiple_of((1 - core) * (count - edge), edge)
+        return remote(
+            gate_buf.at[pl.ds(start, edge), :], halo, halo_sem.at[0], halo_sem.at[1], s, partner
+        )
+
+    halo_copy().start()
+    halo_copy().wait_recv()
+    extra_core = jnp.where(s < extras, 0, 1)
+    extra_tile = jnp.minimum(n_sp + s - extras * extra_core, tiles - 1)
+    slots = ((0, s), (1, s), (extra_core, extra_tile))
+    pos = lax.broadcasted_iota(jnp.int32, (count, LANE), 0)
+    for slot, (block, tile) in enumerate(slots):
+        lane = slice(slot * LANE, (slot + 1) * LANE)
+        tap = taps_all[block, :, lanes(tile, LANE)]
+        g_mid = gate_buf[:, lane].astype(F32)
+        edge_rows = halo[:, lane].astype(F32)
+        before = jnp.where(core == 1, edge_rows[edge - 1 : edge], 0.0)
+        after = jnp.where(core == 0, edge_rows[0:1], 0.0)
+        g_prev = jnp.where(pos == 0, before, pltpu.roll(g_mid, 1, 0))
+        g_next = jnp.where(pos == count - 1, after, pltpu.roll(g_mid, count - 1, 0))
+        conv = tap[0:1] * g_prev + tap[1:2] * g_mid + tap[2:3] * g_next
+        mixed = jax.nn.gelu(conv) * value_buf[:, lane].astype(F32)
+        hidden_buf[:, lane] = mixed.astype(BF16)
+
+    chip_id = s * n_pair + pair
+
+    def r_copy(i):
+        j, m = (i // n_tp, lax.rem(i, n_tp))
+        return j, m, remote(
+            part.at[i], r_all.at[chip_id], r_send.at[i], r_recv.at[chip_id], core * half + j, m
+        )
+
+    def r_index(i):
+        return lax.rem(i + chip_id, half * n_tp)
+
+    def down_block(k):
+        i = r_index(k)
+        j, m, copy = r_copy(i)
+        result = jnp.dot(
+            hidden_buf[rows(j), :], w_down[:, lanes(m, features)], preferred_element_type=F32
+        ).astype(BF16)
+        part[i] = result
+        mine = jnp.logical_and(core * half + j == s, m == t)
+
+        @pl.when(jnp.logical_not(mine))
+        def _():
+            copy.start()
+
+        @pl.when(mine)
+        def _():
+            r_all[chip_id] = result
+
+    loop(0, half * n_tp, down_block)
+
+    out_sum = jnp.zeros((tokens, features), F32)
+    own_core = core == my_half
+    for i in range(n_sp * n_pair):
+        mine = jnp.logical_and(own_core, chip_id == i)
+
+        @pl.when(jnp.logical_not(mine))
+        def _(i=i):
+            remote(part.at[0], r_all.at[i], r_send.at[0], r_recv.at[i], s, partner).wait_recv()
+
+        out_sum = out_sum + r_all[i].astype(F32)
+    out[...] = (stream_own[...].astype(F32) + out_sum).astype(BF16)
+
+    def sent_sp(d):
+        for copy in kv_copies(d) + (g_copy(d),) + weight_copies(d):
+            copy.wait_send()
+
+    loop(1, n_sp, sent_sp)
+
+    def sent_tp(e):
+        wo_copy(e).wait_send()
+        gain_copy(e).wait_send()
+        cell_copy(e).wait_send()
+
+    loop(1, n_tp, sent_tp)
+    taps_copy().wait_send()
+
+    def sent_extra(e):
+        @pl.when(e + extras * core != s)
+        def _():
+            for copy in extra_copies(e, s):
+                copy.wait_send()
+
+    loop(0, extras, sent_extra)
+
+    def sent_x(d):
+        to_s, to_t, copy = x_copy(d)
+
+        @pl.when(jnp.logical_not(jnp.logical_and(to_s == s, to_t == t)))
+        def _():
+            copy.wait_send()
+
+    loop(0, n_sp * n_pair, sent_x)
+    for copy in forward_copies(core, 0):
+        copy.wait_send()
+
+    @pl.when(owner)
+    def _():
+        for copy in forward_copies(2, 2):
+            copy.wait_send()
+
+    halo_copy().wait_send()
+
+    def sent_r(i):
+        j, m, copy = r_copy(i)
+
+        @pl.when(jnp.logical_not(jnp.logical_and(core * half + j == s, m == t)))
+        def _():
+            copy.wait_send()
+
+    loop(0, half * n_tp, sent_r)
+
+
+def fast_layer(n_sp, n_tp, *args):
+    (resid, query, keys, value, gate_logits, gates, extra_logs, head_gain, out_w,
+     mixer_gain, gate_w, value_w, taps, down_w) = args
+    tokens, width = query.shape
+    features = resid.shape[1]
+    model = features * n_tp
+    half = n_sp // 2
+    n_pair = n_tp // 2
+    hidden = 3 * LANE
+    vmem = pl.BlockSpec(memory_space=pltpu.VMEM)
+    anywhere = pl.BlockSpec(memory_space=pl.ANY)
+    dma = pltpu.SemaphoreType.DMA
+    spaces = [vmem, vmem, anywhere, anywhere, vmem, vmem, vmem, vmem, anywhere,
+              vmem, anywhere, anywhere, vmem, anywhere]
+    scratch = [
+        pltpu.VMEM((n_sp * tokens, width), BF16),
+        pltpu.VMEM((n_sp * tokens, width), BF16),
+        pltpu.VMEM((8, tokens), F32),
+        pltpu.VMEM((n_sp, 8, tokens), F32),
+        pltpu.VMEM((8, tokens), F32),
+        pltpu.VMEM((n_tp * width, features), BF16),
+        pltpu.VMEM((2,) + taps.shape, F32),
+        pltpu.VMEM((8, features), F32),
+        pltpu.VMEM((8, model), F32),
+        pltpu.VMEM((3, model, 2 * LANE), BF16),
+        pltpu.VMEM((hidden, model), BF16),
+        pltpu.VMEM((tokens, width), BF16),
+        pltpu.VMEM((n_tp, tokens, width), BF16),
+        pltpu.VMEM((tokens, features), BF16),
+        pltpu.VMEM((half, tokens, model), BF16),
+        pltpu.VMEM((half * tokens, hidden), BF16),
+        pltpu.VMEM((half * tokens, hidden), BF16),
+        pltpu.VMEM((16, hidden), BF16),
+        pltpu.VMEM((half * tokens, hidden), BF16),
+        pltpu.VMEM((half * n_tp, tokens, features), BF16),
+        pltpu.VMEM((n_sp * n_pair, tokens, features), BF16),
+        dma((2, n_sp)),
+        dma((2, n_sp)),
+        dma((2, n_sp)),
+        dma((2, n_tp)),
+        dma((2,)),
+        dma((2, n_tp)),
+        dma((2, n_sp)),
+        dma((2, n_sp)),
+        dma((2, n_sp)),
+        dma((2, n_sp)),
+        dma((2, n_sp)),
+        dma((2, n_sp)),
+        dma((2, 4)),
+        dma((2, n_tp)),
+        dma((n_sp * n_pair,)),
+        dma((half * n_tp,)),
+        dma((2,)),
+        dma((half * n_tp,)),
+        dma((n_sp * n_pair,)),
+        dma((6,)),
+        dma((3,)),
+    ]
+    return pl.pallas_call(
+        functools.partial(layer_kernel, n_sp, n_tp),
+        out_shape=jax.ShapeDtypeStruct((tokens, features), BF16),
+        in_specs=spaces,
+        out_specs=vmem,
+        scratch_shapes=scratch,
+        compiler_params=pltpu.CompilerParams(has_side_effects=True, vmem_limit_bytes=60 * 2**20),
+    )(resid, query, keys, value, gate_logits, gates, extra_logs, head_gain.reshape(1, -1), out_w,
+      mixer_gain.reshape(1, -1), gate_w, value_w, taps, down_w)
+
+
+def choose(n_sp, n_tp, *args):
+    tokens, width = args[1].shape
+    tiles, rest = divmod(args[10].shape[1], LANE)
+    fits = (
+        n_sp % 2 == 0
+        and n_tp % 2 == 0
+        and rest == 0
+        and 0 < tiles - n_sp
+        and 2 * (tiles - n_sp) <= n_sp
+        and tokens == LANE
+        and width == 2 * DH
+        and n_sp * tokens <= 1024
+    )
+    if fits:
+        return fast_layer(n_sp, n_tp, *args)
+    return per_device(*args)
+
+
 def solution(mesh):
     return jax.shard_map(
-        per_device,
+        functools.partial(choose, mesh.shape["sp"], mesh.shape["tp"]),
         mesh=mesh,
         in_specs=(
             P("sp", "tp"),

time: 449 us -> 191 us (0.43)
  the two profiles are of different devices: /device:TPU:29 before, /device:TPU:22 now
where the time goes in v1:
time: 191 us; the launch traced here: 190 us
  Pallas kernels  187 us (98%)
  local copies, waits for them, and re-layouts  3.4 us (2%)
    pallas_call x1, Pallas kernels, fast_layer(): pl.pallas_call(functools.partial(layer_kernel, n_sp, n_tp), out_shape=jax...  187 us

profile of v1, /device:TPU:22, one launch (start us, length us, event | category | flops | bytes accessed | tf_op | source)
XLA Modules:
  0.0 190.4 jit_solution(11615540053788347700)
XLA Ops:
  0.0 0.0 copy-start
  0.0 1.2 reshape.6.head_gain
  1.3 0.0 copy-done
  1.3 0.6 reshape.7.mixer_gain
  1.8 187.0 %shard_map.136 = bf16[128,512]{1,0:T(8,128)(2,1)} custom-call(bf16[128,512]{1,0:T(8,128)(2,1)} %resid.1, bf16[128,256]{1,0:T(8,128)(2,1)} %query.1, bf16[128,256]{1,0:T(8,128)(2,1)} %keys.1, bf16[128,256]{1,0:T(8,128)(2,1)} %value.1, bf16[128,256]{1,0:T(8,128)(2,1)} %gate_logits.1, f32[4,2,128]{2,1,0:T(2,128)} %gates.1, f32[2,2,128]{2,1,0:T(2,128)} %extra_logs.1, ...), custom_call_target="tpu_custom_call" | custom-call | tf_op jit(solution)/shard_map/pallas_call | solution.py:816
  188.8 1.6 copy.16
Async XLA Ops:
  0.0 1.3 copy-start

commit v2 on v1

--- a/solution.py
+++ b/solution.py
@@ -277,6 +277,10 @@
     halo,
     hidden_buf,
     part,
+    part_sum,
+    part_in,
+    sum_in,
+    z_out,
     r_all,
     k_sem,
     v_sem,
@@ -293,9 +297,13 @@
     fwd_sem,
     cell_sem,
     x_send,
+    x_fwd,
+    x_relay,
     x_recv,
     halo_sem,
-    r_send,
+    p_sem,
+    q_sem,
+    z_send,
     r_recv,
     local_sem,
     local_x,
@@ -316,6 +324,10 @@
     half = n_sp // 2
     my_half = s // half
     model = features * n_tp
+    z, y = (s // 2, lax.rem(s, 2))
+    layers = half // 2
+    x_side = (s, 2 * (1 - pair) + core)
+    y_side = (2 * z + 1 - y, t)
 
     def loop(low, high, body):
         def step(i, carry):
@@ -440,24 +452,31 @@
     loop(1, n_tp, start_tp)
     taps_copy().start()
 
-    def start_weights(d):
-        for copy in weight_copies(d):
-            copy.start()
-
-    loop(1, n_sp, start_weights)
-
-    def start_extra(e):
-        @pl.when(e + extras * core != s)
-        def _():
-            for copy in extra_copies(e, s):
+    UP, DOWN = (slice(0, 2), slice(2, 3))
+
+    def start_weights(which):
+        def body(d):
+            for copy in weight_copies(d)[which]:
                 copy.start()
 
-        @pl.when(e + extras * core == s)
-        def _():
-            for copy in local_extra(e):
-                copy.start()
-
-    loop(0, extras, start_extra)
+        loop(1, n_sp, body)
+
+    def start_extras(which):
+        def body(e):
+            @pl.when(e + extras * core != s)
+            def _():
+                for copy in extra_copies(e, s)[which]:
+                    copy.start()
+
+            @pl.when(e + extras * core == s)
+            def _():
+                for copy in local_extra(e)[which]:
+                    copy.start()
+
+        loop(0, extras, body)
+
+    start_weights(UP)
+    start_extras(UP)
 
     loop(1, n_sp, lambda d: g_copy(d).wait_recv())
 
@@ -529,100 +548,127 @@
 
     place = lax.rem(s, half)
 
+    def x_spot(zl, block_y, m):
+        j = 2 * zl + block_y
+        return x_all.at[j, :, lanes(m, features)], j * n_tp + m
+
+    def own_shard(j, m):
+        return jnp.logical_and(core * half + j == s, m == t)
+
     def x_copy(d):
-        chip = lax.rem(s * n_pair + pair + d, n_sp * n_pair)
-        to_s, to_t = (chip // n_pair, 2 * lax.rem(chip, n_pair) + my_half)
-        return to_s, to_t, remote(
-            stream_own,
-            x_all.at[place, :, lanes(t, features)],
-            x_send.at[d],
-            x_recv.at[place * n_tp + t],
-            to_s,
-            to_t,
-        )
+        to_z = lax.rem(z + d, half)
+        spot, index = x_spot(lax.rem(z, layers), y, t)
+        to = (2 * to_z + y, 2 * pair + my_half)
+        return remote(stream_own, spot, x_send.at[d], x_recv.at[index], *to)
+
+    def x_pass(zl, block_y, m, send, to):
+        spot, index = x_spot(zl, block_y, m)
+        return remote(spot, spot, send, x_recv.at[index], *to)
+
+    def stays(d):
+        return jnp.logical_and(d == 0, core == my_half)
 
     def start_x(d):
-        to_s, to_t, copy = x_copy(d)
-        mine = jnp.logical_and(to_s == s, to_t == t)
-
-        @pl.when(jnp.logical_not(mine))
+        @pl.when(jnp.logical_not(stays(d)))
         def _():
-            copy.start()
-
-        @pl.when(mine)
+            x_copy(d).start()
+
+        @pl.when(stays(d))
         def _():
             x_all[place, :, lanes(t, features)] = stream_own[...]
 
-    loop(0, n_sp * n_pair, start_x)
-
-    def wait_weights(d):
-        for copy in weight_copies(d):
+    loop(0, half, start_x)
+    start_weights(DOWN)
+    start_extras(DOWN)
+
+    def column(i):
+        zl, m = (i // 2, 2 * pair + lax.rem(i, 2))
+
+        @pl.when(jnp.logical_not(own_shard(2 * zl + y, m)))
+        def _():
+            x_pass(zl, y, m, x_fwd.at[0, i], x_side).wait_recv()
+
+        x_pass(zl, y, m, x_fwd.at[0, i], x_side).start()
+        x_pass(zl, y, m, x_fwd.at[1, i], y_side).start()
+
+    loop(0, half, column)
+
+    def relays(zl):
+        return (
+            x_pass(zl, y, 2 * (1 - pair), x_relay.at[0, zl], y_side),
+            x_pass(zl, 1 - y, 2 * pair + 1, x_relay.at[1, zl], x_side),
+        )
+
+    def relay(zl):
+        for copy in relays(zl):
             copy.wait_recv()
-
-    loop(1, n_sp, wait_weights)
-    for copy in local_copies()[3:]:
-        copy.wait()
+            copy.start()
+
+    loop(0, layers, relay)
+
+    def wait_weights(which):
+        def body(d):
+            for copy in weight_copies(d)[which]:
+                copy.wait_recv()
+
+        loop(1, n_sp, body)
+
     owner = jnp.logical_and(s >= extras * core, s < extras * (core + 1))
     other_owner = jnp.logical_and(s >= extras * (1 - core), s < extras * (2 - core))
 
-    def forward_copies(slot, base):
-        return (
-            remote(w_up.at[slot], w_up.at[slot], fwd_sem.at[0, base], fwd_sem.at[1, base], s, partner),
-            remote(
-                w_down.at[trows(slot), :],
-                w_down.at[trows(slot), :],
-                fwd_sem.at[0, base + 1],
-                fwd_sem.at[1, base + 1],
-                s,
-                partner,
-            ),
-        )
-
-    for copy in forward_copies(core, 0):
-        copy.start()
-
-    @pl.when(owner)
-    def _():
-        def wait_extra(source):
-            @pl.when(source != s)
-            def _():
-                for copy in extra_copies(0, source):
-                    copy.wait_recv()
-
-        loop(0, n_sp, wait_extra)
-        for copy in local_extra(0):
+    def forward_copy(slot, down):
+        ref = w_down.at[trows(slot), :] if down else w_up.at[slot]
+        at = down + (2 if isinstance(slot, int) else 0)
+        return remote(ref, ref, fwd_sem.at[0, at], fwd_sem.at[1, at], s, partner)
+
+    def pass_on(down):
+        which = DOWN if down else UP
+        wait_weights(which)
+        for copy in local_copies()[3:][which]:
             copy.wait()
-        for copy in forward_copies(2, 2):
-            copy.start()
+        forward_copy(core, down).start()
+
+        @pl.when(owner)
+        def _():
+            def wait_extra(source):
+                @pl.when(source != s)
+                def _():
+                    for copy in extra_copies(0, source)[which]:
+                        copy.wait_recv()
+
+            loop(0, n_sp, wait_extra)
+            for copy in local_extra(0)[which]:
+                copy.wait()
+            forward_copy(2, down).start()
+
+    def take_other(down):
+        forward_copy(1 - core, down).wait_recv()
+
+        @pl.when(other_owner)
+        def _():
+            forward_copy(2, down).wait_recv()
 
     @pl.when(s >= 2 * extras)
     def _():
         w_up[2] = jnp.zeros(w_up.shape[1:], BF16)
         w_down[2 * LANE :, :] = jnp.zeros((LANE, w_down.shape[1]), BF16)
 
-    taps_copy().wait_recv()
-    for copy in forward_copies(1 - core, 0):
-        copy.wait_recv()
-
-    @pl.when(other_owner)
-    def _():
-        for copy in forward_copies(2, 2):
-            copy.wait_recv()
-
-    def mix_block(j):
+    pass_on(0)
+    take_other(0)
+
+    def mix_block(i):
+        zl, side = (lax.rem(i, layers), i // layers)
+        j = 2 * zl + lax.rem(y + side, 2)
         for m in range(n_tp):
-            mine = jnp.logical_and(core * half + j == s, t == m)
-
-            @pl.when(jnp.logical_not(mine))
+            mine = pair == m // 2
+            if m % 2 == 0:
+                seen = side == 0
+            else:
+                seen = mine
+
+            @pl.when(jnp.logical_not(seen))
             def _(m=m):
-                remote(
-                    stream_own,
-                    x_all.at[j, :, pl.ds(m * features, features)],
-                    x_send.at[0],
-                    x_recv.at[j * n_tp + m],
-                    s,
-                    partner,
-                ).wait_recv()
+                x_pass(zl, lax.rem(y + side, 2), m, x_relay.at[0, 0], y_side).wait_recv()
 
         x = x_all[j].astype(F32)
         squares = jnp.sum(x * x, axis=1, keepdims=True)
@@ -645,6 +691,8 @@
         )
 
     halo_copy().start()
+    pass_on(1)
+    taps_copy().wait_recv()
     halo_copy().wait_recv()
     extra_core = jnp.where(s < extras, 0, 1)
     extra_tile = jnp.minimum(n_sp + s - extras * extra_core, tiles - 1)
@@ -663,44 +711,83 @@
         mixed = jax.nn.gelu(conv) * value_buf[:, lane].astype(F32)
         hidden_buf[:, lane] = mixed.astype(BF16)
 
-    chip_id = s * n_pair + pair
-
-    def r_copy(i):
-        j, m = (i // n_tp, lax.rem(i, n_tp))
-        return j, m, remote(
-            part.at[i], r_all.at[chip_id], r_send.at[i], r_recv.at[chip_id], core * half + j, m
-        )
-
-    def r_index(i):
-        return lax.rem(i + chip_id, half * n_tp)
-
-    def down_block(k):
-        i = r_index(k)
-        j, m, copy = r_copy(i)
-        result = jnp.dot(
+    take_other(1)
+
+    def product(j, m):
+        return jnp.dot(
             hidden_buf[rows(j), :], w_down[:, lanes(m, features)], preferred_element_type=F32
-        ).astype(BF16)
-        part[i] = result
-        mine = jnp.logical_and(core * half + j == s, m == t)
-
-        @pl.when(jnp.logical_not(mine))
-        def _():
-            copy.start()
-
-        @pl.when(mine)
-        def _():
-            r_all[chip_id] = result
-
-    loop(0, half * n_tp, down_block)
+        )
+
+    def first_copies(i):
+        return tuple(
+            remote(part.at[k, i], part_in.at[k, i], p_sem.at[0, k, i], p_sem.at[1, k, i], *to)
+            for k, to in enumerate((x_side, y_side))
+        )
+
+    def second_copies(zl):
+        return tuple(
+            remote(
+                part_sum.at[k, zl], sum_in.at[k, zl], q_sem.at[0, k, zl], q_sem.at[1, k, zl], *to
+            )
+            for k, to in enumerate((y_side, x_side))
+        )
+
+    def z_copy(k, zl):
+        to = (2 * (core * layers + zl) + y, 2 * pair + k)
+        mine = jnp.logical_and(to[0] == s, to[1] == t)
+        return mine, remote(z_out.at[k, zl], r_all.at[z], z_send.at[k, zl], r_recv.at[z], *to)
+
+    def first_trip(n):
+        zl, late = (lax.rem(n, layers), n // layers)
+        by = lax.rem(1 - y + late, 2)
+        bx = lax.rem(1 - pair + late, 2)
+        i_x, i_y = (2 * zl + by, 2 * zl + bx)
+        part[0, i_x] = product(2 * zl + by, 2 * (1 - pair)).astype(BF16)
+        first_copies(i_x)[0].start()
+        part[1, i_y] = product(2 * zl + 1 - y, 2 * bx + 1).astype(BF16)
+        first_copies(i_y)[1].start()
+
+    loop(0, half, first_trip)
+
+    def second_trip(zl):
+        i_x, i_y = (2 * zl + 1 - y, 2 * zl + 1 - pair)
+        own = product(2 * zl + 1 - y, 2 * pair)
+        first_copies(i_x)[0].wait_recv()
+        part_sum[0, zl] = (own + part_in[0, i_x].astype(F32)).astype(BF16)
+        second_copies(zl)[0].start()
+        own = product(2 * zl + y, 2 * (1 - pair) + 1)
+        first_copies(i_y)[1].wait_recv()
+        part_sum[1, zl] = (own + part_in[1, i_y].astype(F32)).astype(BF16)
+        second_copies(zl)[1].start()
+
+    loop(0, layers, second_trip)
+
+    def third_trip(zl):
+        for k, i in enumerate((2 * zl + y, 2 * zl + pair)):
+            own = product(2 * zl + y, 2 * pair + k)
+            first_copies(i)[k].wait_recv()
+            own = own + part_in[k, i].astype(F32)
+            second_copies(zl)[k].wait_recv()
+            result = (own + sum_in[k, zl].astype(F32)).astype(BF16)
+            z_out[k, zl] = result
+            mine, copy = z_copy(k, zl)
+
+            @pl.when(jnp.logical_not(mine))
+            def _():
+                copy.start()
+
+            @pl.when(mine)
+            def _():
+                r_all[z] = result
+
+    loop(0, layers, third_trip)
 
     out_sum = jnp.zeros((tokens, features), F32)
-    own_core = core == my_half
-    for i in range(n_sp * n_pair):
-        mine = jnp.logical_and(own_core, chip_id == i)
-
-        @pl.when(jnp.logical_not(mine))
+    for i in range(half):
+
+        @pl.when(jnp.logical_not(jnp.logical_and(core == my_half, z == i)))
         def _(i=i):
-            remote(part.at[0], r_all.at[i], r_send.at[0], r_recv.at[i], s, partner).wait_recv()
+            remote(z_out.at[0, 0], r_all.at[i], z_send.at[0, 0], r_recv.at[i], *y_side).wait_recv()
 
         out_sum = out_sum + r_all[i].astype(F32)
     out[...] = (stream_own[...].astype(F32) + out_sum).astype(BF16)
@@ -728,31 +815,37 @@
     loop(0, extras, sent_extra)
 
     def sent_x(d):
-        to_s, to_t, copy = x_copy(d)
-
-        @pl.when(jnp.logical_not(jnp.logical_and(to_s == s, to_t == t)))
+        @pl.when(jnp.logical_not(stays(d)))
         def _():
+            x_copy(d).wait_send()
+
+        for k, to in enumerate((x_side, y_side)):
+            x_pass(d // 2, y, 2 * pair + lax.rem(d, 2), x_fwd.at[k, d], to).wait_send()
+        for copy in first_copies(d):
             copy.wait_send()
 
-    loop(0, n_sp * n_pair, sent_x)
-    for copy in forward_copies(core, 0):
-        copy.wait_send()
+    loop(0, half, sent_x)
+
+    def sent_layer(zl):
+        for copy in relays(zl) + second_copies(zl):
+            copy.wait_send()
+        for k in range(2):
+            mine, copy = z_copy(k, zl)
+
+            @pl.when(jnp.logical_not(mine))
+            def _(copy=copy):
+                copy.wait_send()
+
+    loop(0, layers, sent_layer)
+    for down in range(2):
+        forward_copy(core, down).wait_send()
 
     @pl.when(owner)
     def _():
-        for copy in forward_copies(2, 2):
-            copy.wait_send()
+        for down in range(2):
+            forward_copy(2, down).wait_send()
 
     halo_copy().wait_send()
-
-    def sent_r(i):
-        j, m, copy = r_copy(i)
-
-        @pl.when(jnp.logical_not(jnp.logical_and(core * half + j == s, m == t)))
-        def _():
-            copy.wait_send()
-
-    loop(0, half * n_tp, sent_r)
 
 
 def fast_layer(n_sp, n_tp, *args):
@@ -789,8 +882,12 @@
         pltpu.VMEM((half * tokens, hidden), BF16),
         pltpu.VMEM((16, hidden), BF16),
         pltpu.VMEM((half * tokens, hidden), BF16),
-        pltpu.VMEM((half * n_tp, tokens, features), BF16),
-        pltpu.VMEM((n_sp * n_pair, tokens, features), BF16),
+        pltpu.VMEM((2, half, tokens, features), BF16),
+        pltpu.VMEM((2, half // 2, tokens, features), BF16),
+        pltpu.VMEM((2, half, tokens, features), BF16),
+        pltpu.VMEM((2, half // 2, tokens, features), BF16),
+        pltpu.VMEM((2, half // 2, tokens, features), BF16),
+        pltpu.VMEM((half, tokens, features), BF16),
         dma((2, n_sp)),
         dma((2, n_sp)),
         dma((2, n_sp)),
@@ -805,11 +902,15 @@
         dma((2, n_sp)),
         dma((2, 4)),
         dma((2, n_tp)),
-        dma((n_sp * n_pair,)),
+        dma((half,)),
+        dma((2, half)),
+        dma((2, half // 2)),
         dma((half * n_tp,)),
         dma((2,)),
-        dma((half * n_tp,)),
-        dma((n_sp * n_pair,)),
+        dma((2, 2, half)),
+        dma((2, 2, half // 2)),
+        dma((2, half // 2)),
+        dma((half,)),
         dma((6,)),
         dma((3,)),
     ]
@@ -829,7 +930,8 @@
     tiles, rest = divmod(args[10].shape[1], LANE)
     fits = (
         n_sp % 2 == 0
-        and n_tp % 2 == 0
+        and n_sp % 4 == 0
+        and n_tp == 4
         and rest == 0
         and 0 < tiles - n_sp
         and 2 * (tiles - n_sp) <= n_sp

time: 191 us -> 141 us (0.74)
  the two profiles are of different devices: /device:TPU:22 before, /device:TPU:29 now
where the time goes in v2:
time: 141 us; the launch traced here: 140 us
  Pallas kernels  137 us (97%)
  local copies, waits for them, and re-layouts  3.4 us (2%)
    pallas_call x1, Pallas kernels, fast_layer(): pl.pallas_call(functools.partial(layer_kernel, n_sp, n_tp), out_shape=jax...  137 us

profile of v2, /device:TPU:29, one launch (start us, length us, event | category | flops | bytes accessed | tf_op | source)
XLA Modules:
  0.0 140.4 jit_solution(14996014027472358334)
XLA Ops:
  0.0 0.0 copy-start
  0.0 1.2 reshape.6.head_gain
  1.3 0.0 copy-done
  1.3 0.6 reshape.7.mixer_gain
  1.8 137.0 %shard_map.136 = bf16[128,512]{1,0:T(8,128)(2,1)} custom-call(bf16[128,512]{1,0:T(8,128)(2,1)} %resid.1, bf16[128,256]{1,0:T(8,128)(2,1)} %query.1, bf16[128,256]{1,0:T(8,128)(2,1)} %keys.1, bf16[128,256]{1,0:T(8,128)(2,1)} %value.1, bf16[128,256]{1,0:T(8,128)(2,1)} %gate_logits.1, f32[4,2,128]{2,1,0:T(2,128)} %gates.1, f32[2,2,128]{2,1,0:T(2,128)} %extra_logs.1, ...), custom_call_target="tpu_custom_call" | custom-call | tf_op jit(solution)/shard_map/pallas_call | solution.py:917
  138.9 1.6 %copy.16 = bf16[128,512]{1,0:T(8,128)(2,1)} copy(bf16[128,512]{1,0:T(8,128)(2,1)} %shard_map.136) | data formatting | bytes 262144
Async XLA Ops:
  0.0 1.3 copy-start

commit v3 on v2

--- a/solution.py
+++ b/solution.py
@@ -412,6 +412,16 @@
             for i, (a, b) in enumerate(tile_ends(n_sp + e, 2))
         )
 
+    barrier = pltpu.get_barrier_semaphore()
+
+    def greet(to_s, to_t):
+        pl.semaphore_signal(barrier, inc=1, device_id=(to_s, to_t), device_id_type=MESH)
+
+    loop(1, n_sp, lambda d: greet(lax.rem(s + d, n_sp), t))
+    loop(1, n_tp, lambda e: greet(s, lax.rem(t + e, n_tp)))
+    loop(1, half, lambda d: greet(2 * lax.rem(z + d, half) + y, partner))
+    pl.semaphore_wait(barrier, n_sp + n_tp + half - 3)
+
     def start_kv(d):
         for copy in kv_copies(d):
             copy.start()
@@ -920,7 +930,7 @@
         in_specs=spaces,
         out_specs=vmem,
         scratch_shapes=scratch,
-        compiler_params=pltpu.CompilerParams(has_side_effects=True, vmem_limit_bytes=60 * 2**20),
+        compiler_params=pltpu.CompilerParams(has_side_effects=True, collective_id=0, vmem_limit_bytes=60 * 2**20),
     )(resid, query, keys, value, gate_logits, gates, extra_logs, head_gain.reshape(1, -1), out_w,
       mixer_gain.reshape(1, -1), gate_w, value_w, taps, down_w)
 

time: 141 us -> 137 us (0.972)
  Pallas kernels: 137 us -> 133 us
    pallas_call x1, Pallas kernels: 137 us -> 133 us  [fast_layer(): pl.pallas_call(functools.partial(layer_kernel, n_sp, n_tp), out_shape=jax...]
where the time goes in v3:
time: 137 us; the launch traced here: 136 us
  Pallas kernels  133 us (97%)
  local copies, waits for them, and re-layouts  3.4 us (2%)
    pallas_call x1, Pallas kernels, fast_layer(): pl.pallas_call(functools.partial(layer_kernel, n_sp, n_tp), out_shape=jax...  133 us

profile of v3, /device:TPU:29, one launch (start us, length us, event | category | flops | bytes accessed | tf_op | source)
XLA Modules:
  0.0 136.2 jit_solution(7601353176232421935)
XLA Ops:
  0.0 0.0 copy-start
  0.0 1.2 reshape.6.head_gain
  1.3 0.0 copy-done
  1.3 0.6 reshape.7.mixer_gain
  1.8 132.7 %shard_map.136 = bf16[128,512]{1,0:T(8,128)(2,1)} custom-call(bf16[128,512]{1,0:T(8,128)(2,1)} %resid.1, bf16[128,256]{1,0:T(8,128)(2,1)} %query.1, bf16[128,256]{1,0:T(8,128)(2,1)} %keys.1, bf16[128,256]{1,0:T(8,128)(2,1)} %value.1, bf16[128,256]{1,0:T(8,128)(2,1)} %gate_logits.1, f32[4,2,128]{2,1,0:T(2,128)} %gates.1, f32[2,2,128]{2,1,0:T(2,128)} %extra_logs.1, ...), custom_call_target="tpu_custom_call" | custom-call | tf_op jit(solution)/shard_map/pallas_call | solution.py:927
  134.6 1.6 %copy.16 = bf16[128,512]{1,0:T(8,128)(2,1)} copy(bf16[128,512]{1,0:T(8,128)(2,1)} %shard_map.136) | data formatting | bytes 262144
Async XLA Ops:
  0.0 1.3 copy-start

commit v4 on v3

--- a/solution.py
+++ b/solution.py
@@ -342,10 +342,21 @@
     trows = lambda i: pl.ds(pl.multiple_of(i * LANE, LANE), LANE)
 
     def kv_copies(d):
-        to = lax.rem(s + d, n_sp)
+        to = (lax.rem(2 * d + s, n_sp), t)
+        return kv_pair((keys, value), s, d, to)
+
+    def kv_side():
+        return kv_pair((keys, value), s, 0, y_side)
+
+    def kv_relay(d):
+        source = lax.rem(s - 2 * d + n_sp, n_sp)
+        at = rows(source)
+        return kv_pair((k_all.at[at, :], v_all.at[at, :]), source, half + d, y_side)
+
+    def kv_pair(refs, source, at, to):
         return (
-            remote(keys, k_all.at[rows(s), :], k_sem.at[0, d], k_sem.at[1, d], to, t),
-            remote(value, v_all.at[rows(s), :], v_sem.at[0, d], v_sem.at[1, d], to, t),
+            remote(refs[0], k_all.at[rows(source), :], k_sem.at[0, at], k_sem.at[1, at], *to),
+            remote(refs[1], v_all.at[rows(source), :], v_sem.at[0, at], v_sem.at[1, at], *to),
         )
 
     def g_copy(d):
@@ -426,7 +437,9 @@
         for copy in kv_copies(d):
             copy.start()
 
-    loop(1, n_sp, start_kv)
+    for copy in kv_side():
+        copy.start()
+    loop(1, half, start_kv)
     for copy in local_copies():
         copy.start()
 
@@ -449,7 +462,7 @@
     g_own[0:heads, :] = gates[0] - row_incl[0:heads]
     g_own[heads : 2 * heads, :] = gates[2] + row_excl[heads : 2 * heads]
     g_own[2 * heads : 4 * heads, :] = total[0 : 2 * heads]
-    gain_own[...] = jnp.broadcast_to(mixer_gain[...].astype(F32), gain_own.shape)
+    gain_own[...] = jnp.broadcast_to(mixer_gain[...].astype(F32).reshape(1, features), gain_own.shape)
     g_all[s] = g_own[...]
     gain_all[:, lanes(t, features)] = gain_own[...]
     taps_all[core] = taps[...]
@@ -462,7 +475,8 @@
     loop(1, n_tp, start_tp)
     taps_copy().start()
 
-    UP, DOWN = (slice(0, 2), slice(2, 3))
+    GATE, VALUE, DOWN = (slice(0, 1), slice(1, 2), slice(2, 3))
+    KINDS = (GATE, VALUE, DOWN)
 
     def start_weights(which):
         def body(d):
@@ -485,13 +499,20 @@
 
         loop(0, extras, body)
 
-    start_weights(UP)
-    start_extras(UP)
+    start_weights(GATE)
+    start_extras(GATE)
+
+    def pass_kv(d):
+        for copy, onward in zip(kv_copies(d), kv_relay(d)):
+            copy.wait_recv()
+            onward.start()
+
+    loop(1, half, pass_kv)
 
     loop(1, n_sp, lambda d: g_copy(d).wait_recv())
 
     def wait_kv(d):
-        for copy in kv_copies(d):
+        for copy in kv_relay(d):
             copy.wait_recv()
 
     for copy in local_copies()[:3]:
@@ -522,7 +543,10 @@
         logs.append(
             jnp.concatenate([jnp.exp(f - peak) + jnp.exp(b - peak) for f, b in logs_h], axis=1)
         )
-    loop(1, n_sp, wait_kv)
+    for copy in kv_side():
+        copy.wait_recv()
+    loop(1, half, wait_kv)
+    head_row = head_gain[...].astype(F32).reshape(1, width)
     for h in range(heads):
         lane = slice(h * DH, (h + 1) * DH)
         scores = nt_dot(query[:, lane], k_all[:, lane]) * DH ** (-0.5)
@@ -530,7 +554,7 @@
         numer = jnp.dot(weighted, v_all[:, lane], preferred_element_type=F32)
         scale = lax.rsqrt(jnp.mean(numer * numer, axis=1, keepdims=True) + EPS)
         gated = (
-            numer * scale * head_gain[:, lane].astype(F32)
+            numer * scale * head_row[:, lane]
             * jax.nn.sigmoid(gate_logits[:, lane].astype(F32))
         )
         cell_own[:, lane] = gated.astype(BF16)
@@ -556,66 +580,6 @@
         projected = projected + piece.astype(BF16).astype(F32)
     stream_own[...] = (resid[...].astype(F32) + projected).astype(BF16)
 
-    place = lax.rem(s, half)
-
-    def x_spot(zl, block_y, m):
-        j = 2 * zl + block_y
-        return x_all.at[j, :, lanes(m, features)], j * n_tp + m
-
-    def own_shard(j, m):
-        return jnp.logical_and(core * half + j == s, m == t)
-
-    def x_copy(d):
-        to_z = lax.rem(z + d, half)
-        spot, index = x_spot(lax.rem(z, layers), y, t)
-        to = (2 * to_z + y, 2 * pair + my_half)
-        return remote(stream_own, spot, x_send.at[d], x_recv.at[index], *to)
-
-    def x_pass(zl, block_y, m, send, to):
-        spot, index = x_spot(zl, block_y, m)
-        return remote(spot, spot, send, x_recv.at[index], *to)
-
-    def stays(d):
-        return jnp.logical_and(d == 0, core == my_half)
-
-    def start_x(d):
-        @pl.when(jnp.logical_not(stays(d)))
-        def _():
-            x_copy(d).start()
-
-        @pl.when(stays(d))
-        def _():
-            x_all[place, :, lanes(t, features)] = stream_own[...]
-
-    loop(0, half, start_x)
-    start_weights(DOWN)
-    start_extras(DOWN)
-
-    def column(i):
-        zl, m = (i // 2, 2 * pair + lax.rem(i, 2))
-
-        @pl.when(jnp.logical_not(own_shard(2 * zl + y, m)))
-        def _():
-            x_pass(zl, y, m, x_fwd.at[0, i], x_side).wait_recv()
-
-        x_pass(zl, y, m, x_fwd.at[0, i], x_side).start()
-        x_pass(zl, y, m, x_fwd.at[1, i], y_side).start()
-
-    loop(0, half, column)
-
-    def relays(zl):
-        return (
-            x_pass(zl, y, 2 * (1 - pair), x_relay.at[0, zl], y_side),
-            x_pass(zl, 1 - y, 2 * pair + 1, x_relay.at[1, zl], x_side),
-        )
-
-    def relay(zl):
-        for copy in relays(zl):
-            copy.wait_recv()
-            copy.start()
-
-    loop(0, layers, relay)
-
     def wait_weights(which):
         def body(d):
             for copy in weight_copies(d)[which]:
@@ -627,12 +591,15 @@
     other_owner = jnp.logical_and(s >= extras * (1 - core), s < extras * (2 - core))
 
     def forward_copy(slot, down):
-        ref = w_down.at[trows(slot), :] if down else w_up.at[slot]
-        at = down + (2 if isinstance(slot, int) else 0)
+        if down == 2:
+            ref = w_down.at[trows(slot), :]
+        else:
+            ref = w_up.at[slot, :, pl.ds(down * LANE, LANE)]
+        at = down + (3 if isinstance(slot, int) else 0)
         return remote(ref, ref, fwd_sem.at[0, at], fwd_sem.at[1, at], s, partner)
 
     def pass_on(down):
-        which = DOWN if down else UP
+        which = KINDS[down]
         wait_weights(which)
         for copy in local_copies()[3:][which]:
             copy.wait()
@@ -658,13 +625,77 @@
         def _():
             forward_copy(2, down).wait_recv()
 
+    place = lax.rem(s, half)
+
+    def x_spot(zl, block_y, m):
+        j = 2 * zl + block_y
+        return x_all.at[j, :, lanes(m, features)], j * n_tp + m
+
+    def own_shard(j, m):
+        return jnp.logical_and(core * half + j == s, m == t)
+
+    def x_copy(d):
+        to_z = lax.rem(z + d, half)
+        spot, index = x_spot(lax.rem(z, layers), y, t)
+        to = (2 * to_z + y, 2 * pair + my_half)
+        return remote(stream_own, spot, x_send.at[d], x_recv.at[index], *to)
+
+    def x_pass(zl, block_y, m, send, to):
+        spot, index = x_spot(zl, block_y, m)
+        return remote(spot, spot, send, x_recv.at[index], *to)
+
+    def stays(d):
+        return jnp.logical_and(d == 0, core == my_half)
+
+    def start_x(d):
+        @pl.when(jnp.logical_not(stays(d)))
+        def _():
+            x_copy(d).start()
+
+        @pl.when(stays(d))
+        def _():
+            x_all[place, :, lanes(t, features)] = stream_own[...]
+
+    loop(0, half, start_x)
+    start_weights(VALUE)
+    start_extras(VALUE)
+    start_weights(DOWN)
+    start_extras(DOWN)
+    pass_on(0)
+
+    def column(i):
+        zl, m = (i // 2, 2 * pair + lax.rem(i, 2))
+
+        @pl.when(jnp.logical_not(own_shard(2 * zl + y, m)))
+        def _():
+            x_pass(zl, y, m, x_fwd.at[0, i], x_side).wait_recv()
+
+        x_pass(zl, y, m, x_fwd.at[0, i], x_side).start()
+        x_pass(zl, y, m, x_fwd.at[1, i], y_side).start()
+
+    loop(0, half, column)
+
+    def relays(zl):
+        return (
+            x_pass(zl, y, 2 * (1 - pair), x_relay.at[0, zl], y_side),
+            x_pass(zl, 1 - y, 2 * pair + 1, x_relay.at[1, zl], x_side),
+        )
+
+    def relay(zl):
+        for copy in relays(zl):
+            copy.wait_recv()
+            copy.start()
+
+    loop(0, layers, relay)
+
     @pl.when(s >= 2 * extras)
     def _():
         w_up[2] = jnp.zeros(w_up.shape[1:], BF16)
         w_down[2 * LANE :, :] = jnp.zeros((LANE, w_down.shape[1]), BF16)
 
-    pass_on(0)
+    pass_on(1)
     take_other(0)
+    take_other(1)
 
     def mix_block(i):
         zl, side = (lax.rem(i, layers), i // layers)
@@ -701,7 +732,7 @@
         )
 
     halo_copy().start()
-    pass_on(1)
+    pass_on(2)
     taps_copy().wait_recv()
     halo_copy().wait_recv()
     extra_core = jnp.where(s < extras, 0, 1)
@@ -721,7 +752,7 @@
         mixed = jax.nn.gelu(conv) * value_buf[:, lane].astype(F32)
         hidden_buf[:, lane] = mixed.astype(BF16)
 
-    take_other(1)
+    take_other(2)
 
     def product(j, m):
         return jnp.dot(
@@ -803,10 +834,18 @@
     out[...] = (stream_own[...].astype(F32) + out_sum).astype(BF16)
 
     def sent_sp(d):
-        for copy in kv_copies(d) + (g_copy(d),) + weight_copies(d):
+        for copy in (g_copy(d),) + weight_copies(d):
             copy.wait_send()
 
     loop(1, n_sp, sent_sp)
+    for copy in kv_side():
+        copy.wait_send()
+
+    def sent_kv(d):
+        for copy in kv_copies(d) + kv_relay(d):
+            copy.wait_send()
+
+    loop(1, half, sent_kv)
 
     def sent_tp(e):
         wo_copy(e).wait_send()
@@ -847,12 +886,12 @@
                 copy.wait_send()
 
     loop(0, layers, sent_layer)
-    for down in range(2):
+    for down in range(3):
         forward_copy(core, down).wait_send()
 
     @pl.when(owner)
     def _():
-        for down in range(2):
+        for down in range(3):
             forward_copy(2, down).wait_send()
 
     halo_copy().wait_send()
@@ -910,7 +949,7 @@
         dma((2, n_sp)),
         dma((2, n_sp)),
         dma((2, n_sp)),
-        dma((2, 4)),
+        dma((2, n_sp)),
         dma((2, n_tp)),
         dma((half,)),
         dma((2, half)),
@@ -931,8 +970,8 @@
         out_specs=vmem,
         scratch_shapes=scratch,
         compiler_params=pltpu.CompilerParams(has_side_effects=True, collective_id=0, vmem_limit_bytes=60 * 2**20),
-    )(resid, query, keys, value, gate_logits, gates, extra_logs, head_gain.reshape(1, -1), out_w,
-      mixer_gain.reshape(1, -1), gate_w, value_w, taps, down_w)
+    )(resid, query, keys, value, gate_logits, gates, extra_logs, head_gain, out_w,
+      mixer_gain, gate_w, value_w, taps, down_w)
 
 
 def choose(n_sp, n_tp, *args):

time: 137 us -> 115 us (0.84)
  Pallas kernels: 133 us -> 113 us
  local copies, waits for them, and re-layouts: 3.4 us -> 1.57 us
    pallas_call x1, Pallas kernels: 133 us -> 113 us  [fast_layer(): pl.pallas_call(functools.partial(layer_kernel, n_sp, n_tp), out_shape=jax...]
    reshape x2 -> x0, local copies, waits for them, and re-layouts: 1.83 us -> none  [the longest x1 1.25 us: fast_layer(): head_gain.reshape(1, -1)]
where the time goes in v4:
time: 115 us
  Pallas kernels  113 us (98%)
  local copies, waits for them, and re-layouts  1.57 us (1%)
    pallas_call x1, Pallas kernels, fast_layer(): pl.pallas_call(functools.partial(layer_kernel, n_sp, n_tp), out_shape=jax...  113 us

profile of v4, /device:TPU:29, one launch (start us, length us, event | category | flops | bytes accessed | tf_op | source)
XLA Modules:
  0.0 114.9 jit_solution(16224082966462723396)
XLA Ops:
  0.0 113.4 %shard_map.136 = bf16[128,512]{1,0:T(8,128)(2,1)} custom-call(bf16[128,512]{1,0:T(8,128)(2,1)} %resid.1, bf16[128,256]{1,0:T(8,128)(2,1)} %query.1, bf16[128,256]{1,0:T(8,128)(2,1)} %keys.1, bf16[128,256]{1,0:T(8,128)(2,1)} %value.1, bf16[128,256]{1,0:T(8,128)(2,1)} %gate_logits.1, f32[4,2,128]{2,1,0:T(2,128)} %gates.1, f32[2,2,128]{2,1,0:T(2,128)} %extra_logs.1, ...), custom_call_target="tpu_custom_call" | custom-call | tf_op jit(solution)/shard_map/pallas_call | solution.py:966
  113.4 1.6 %copy.16 = bf16[128,512]{1,0:T(8,128)(2,1)} copy(bf16[128,512]{1,0:T(8,128)(2,1)} %shard_map.136) | data formatting | bytes 262144
